TPU v7x, 32 devices: a whole 2x2x4 slice. The times are simulated.
32 devices in a mesh: fs: 8 (over z, x), tp: 4 (over y, core).
Axes of the slice: x: 2, y: 2, z: 4, core: 2. Of those that a mesh axis runs over, the one named last changes fastest.
Arguments:
- saved_input: bfloat16 [20480, 2048], P('fs'), may hold values from -6 to 6
- value_cot: bfloat16 [20480, 1024], P('fs', 'tp'), may hold values from -6 to 6
- query_cot: bfloat16 [20480, 512], P('fs', 'tp'), may hold values from -6 to 6
- value_master: float32 [2048, 1024], P('fs', 'tp'), may hold values from -0.125 to 0.125
- query_master: float32 [2048, 512], P('fs', 'tp'), may hold values from -0.125 to 0.125
- value_factor: bfloat16 [2048, 256], P('fs'), may hold values from -0.125 to 0.125
- query_factor: bfloat16 [2048, 256], P('fs'), may hold values from -0.125 to 0.125
- value_first: float32 [256, 1024], P('fs', 'tp'), as said below
- value_second: float32 [256, 1024], P('fs', 'tp'), as said below
- query_first: float32 [256, 512], P('fs', 'tp'), as said below
- query_second: float32 [256, 512], P('fs', 'tp'), as said below
Outputs:
- value_step: float32 [2048, 1024], P('fs', 'tp')
- query_step: float32 [2048, 512], P('fs', 'tp')
- value_master_new: float32 [2048, 1024], P('fs', 'tp')
- query_master_new: float32 [2048, 512], P('fs', 'tp')
- value_copy: bfloat16 [2048, 1024], P(None, 'tp')
- query_copy: bfloat16 [2048, 512], P(None, 'tp')
- value_first_new: float32 [256, 1024], P('fs', 'tp')
- value_second_new: float32 [256, 1024], P('fs', 'tp')
- query_first_new: float32 [256, 512], P('fs', 'tp')
- query_second_new: float32 [256, 512], P('fs', 'tp')
Inputs may be any that keep to these rules, and one draw needn't show every extreme that they name: `value_first`: first moments are real-valued of the projected gradient's order. `value_second`: second moments are positive. `query_first`: first moments are real-valued of the projected gradient's order. `query_second`: second moments are positive.
All inputs are finite; a program needn't handle non-finite values.
Results may differ from a plain program's by a relative error of at most 0.001.
Values may be sent and summed in bfloat16 or wider, within the bound.
A program may use at most 64 MiB of HBM per device.

v0:
```python
import jax
import jax.numpy as jnp
from jax import lax
from jax.sharding import PartitionSpec as P

RANK = 256
V_W = 1024
QK_W = 512
BETA_ONE = 0.9
BETA_TWO = 0.95
DENOM_EPS = 1e-08
NORM_EPS = 1e-06
STEP_SIZE = 0.05


def moment_update(projected, first, second):
    first_new = BETA_ONE * first + (1.0 - BETA_ONE) * projected
    second_new = BETA_TWO * second + (1.0 - BETA_TWO) * projected * projected
    direction = first_new / (jnp.sqrt(second_new) + DENOM_EPS)
    return (first_new, second_new, direction)


def on_device(
    saved_input,
    value_cot,
    query_cot,
    value_master,
    query_master,
    value_factor,
    query_factor,
    value_first,
    value_second,
    query_first,
    query_second,
):
    shards = lax.axis_size("fs")
    tokens_all = saved_input.shape[0] * shards
    highest = lax.Precision.HIGHEST
    value_reduced = jnp.dot(
        saved_input,
        lax.all_gather(value_factor, "fs", axis=0, tiled=True),
        preferred_element_type=jnp.float32,
    )
    query_reduced = jnp.dot(
        saved_input,
        lax.all_gather(query_factor, "fs", axis=0, tiled=True),
        preferred_element_type=jnp.float32,
    )
    value_part = (
        lax.dot_general(
            value_reduced,
            value_cot.astype(jnp.float32),
            (((0,), (0,)), ((), ())),
            precision=highest,
        )
        / tokens_all
    )
    query_part = (
        lax.dot_general(
            query_reduced,
            query_cot.astype(jnp.float32),
            (((0,), (0,)), ((), ())),
            precision=highest,
        )
        / tokens_all
    )
    value_share, query_share = (
        lax.psum_scatter(value_part, "fs", scatter_dimension=0, tiled=True),
        lax.psum_scatter(query_part, "fs", scatter_dimension=0, tiled=True),
    )
    value_first_new, value_second_new, value_dir_own = moment_update(
        value_share, value_first, value_second
    )
    query_first_new, query_second_new, query_dir_own = moment_update(
        query_share, query_first, query_second
    )
    value_direction, query_direction = (
        lax.all_gather(value_dir_own, "fs", axis=0, tiled=True),
        lax.all_gather(query_dir_own, "fs", axis=0, tiled=True),
    )
    square_sum = lax.psum(
        jnp.sum(value_dir_own * value_dir_own) + jnp.sum(query_dir_own * query_dir_own),
        ("fs", "tp"),
    )
    update_scale = 1.0 / jnp.sqrt(square_sum / (RANK * (V_W + QK_W)) + NORM_EPS)
    value_step = (
        jnp.dot(value_factor.astype(jnp.float32), value_direction, precision=highest) * update_scale
    )
    query_step = (
        jnp.dot(query_factor.astype(jnp.float32), query_direction, precision=highest) * update_scale
    )
    value_master_new = value_master - STEP_SIZE * value_step
    query_master_new = query_master - STEP_SIZE * query_step
    value_copy, query_copy = (
        lax.all_gather(value_master_new.astype(jnp.bfloat16), "fs", axis=0, tiled=True),
        lax.all_gather(query_master_new.astype(jnp.bfloat16), "fs", axis=0, tiled=True),
    )
    return (
        value_step,
        query_step,
        value_master_new,
        query_master_new,
        value_copy,
        query_copy,
        value_first_new,
        value_second_new,
        query_first_new,
        query_second_new,
    )


def solution(mesh):
    in_specs = (
        P("fs", None),
        P("fs", "tp"),
        P("fs", "tp"),
        P("fs", "tp"),
        P("fs", "tp"),
        P("fs", None),
        P("fs", None),
        P("fs", "tp"),
        P("fs", "tp"),
        P("fs", "tp"),
        P("fs", "tp"),
    )
    out_specs = (
        P("fs", "tp"),
        P("fs", "tp"),
        P("fs", "tp"),
        P("fs", "tp"),
        P(None, "tp"),
        P(None, "tp"),
        P("fs", "tp"),
        P("fs", "tp"),
        P("fs", "tp"),
        P("fs", "tp"),
    )
    return jax.shard_map(
        on_device, mesh=mesh, in_specs=in_specs, out_specs=out_specs, check_vma=False
    )
```

profile of v0, /device:TPU:0, one launch (start us, length us, event | category | flops | bytes accessed | tf_op | source)
XLA Modules:
  0.0 375.6 jit_solution(1386011810459708542)
XLA Ops:
  7.2 0.0 copy-start
  7.2 0.0 all-gather.6.cloned.1.call-start
  7.2 0.7 all-gather.6.cloned.1.call-update
  7.9 0.0 all-gather.4.cloned.1.call-start
  8.0 0.7 all-gather.4.cloned.1.call-update
  8.7 0.0 copy-start.1
  8.7 0.0 reduce-scatter.5.cloned.1.call-start
  8.7 44.4 %all-gather.6.cloned.1.call-done = bf16[2048,256]{1,0:T(8,128)(2,1)} async-done(((bf16[256,256]{1,0:T(8,128)(2,1)}), bf16[2048,256]{1,0:T(8,128)(2,1)}) %all-gather.6.cloned.1.call-update) | async-done | bytes 1048592 | tf_op jit(solution)/shard_map/all_gather | solution.py:46
  53.2 5.9 %fusion.9 = f32[2560,256]{1,0:T(8,128)S(1)} fusion(bf16[2560,2048]{1,0:T(8,128)(2,1)} %param.11, bf16[2048,256]{1,0:T(8,128)(2,1)} %all-gather.6.cloned.1.call-done), kind=kOutput, calls=%fused_computation.21 | convolution fusion | flops 2684354560 | bytes 14155776 | tf_op jit(solution)/shard_map/dot_general | solution.py:44
  59.1 0.0 copy-done.1
  59.1 2.9 convolution_multiply_fusion.3
  61.9 0.0 reduce-scatter.5.cloned.1.call-update
  62.0 0.0 reduce-scatter.3.cloned.1.call-start
  62.0 32.3 %all-gather.4.cloned.1.call-done = bf16[2048,256]{1,0:T(8,128)(2,1)} async-done(((bf16[256,256]{1,0:T(8,128)(2,1)}), bf16[2048,256]{1,0:T(8,128)(2,1)}) %all-gather.4.cloned.1.call-update) | async-done | bytes 1048592 | tf_op jit(solution)/shard_map/all_gather | solution.py:41
  94.3 5.9 %fusion.8 = f32[2560,256]{1,0:T(8,128)S(1)} fusion(bf16[2560,2048]{1,0:T(8,128)(2,1)} %param.11, bf16[2048,256]{1,0:T(8,128)(2,1)} %all-gather.4.cloned.1.call-done), kind=kOutput, calls=%fused_computation.20 | convolution fusion | flops 2684354560 | bytes 14155776 | tf_op jit(solution)/shard_map/dot_general | solution.py:39
  100.2 0.0 copy-done
  100.2 0.0 copy-start.8
  100.2 0.0 copy-start.9
  100.2 0.0 copy-start.6
  100.3 0.0 copy-start.7
  100.3 0.0 copy-start.4
  100.3 0.0 copy-start.2
  100.3 0.0 copy-start.5
  100.3 2.9 convolution_multiply_fusion.1
  103.2 0.0 reduce-scatter.3.cloned.1.call-update
  103.3 0.0 all-gather.8.cloned.1.call-start
  103.3 55.4 %reduce-scatter.5.cloned.1.call-done = f32[32,128]{1,0:T(8,128)} async-done(((f32[256,128]{1,0:T(8,128)}), f32[32,128]{1,0:T(8,128)}) %reduce-scatter.5.cloned.1.call-update) | async-done | bytes 16400 | tf_op jit(solution)/shard_map/reduce_scatter | solution.py:69
  158.7 0.0 copy-done.8
  158.7 0.0 copy-done.9
  158.7 1.9 multiply_reduce_fusion.1
  160.7 63.0 %reduce-scatter.3.cloned.1.call-done = f32[32,256]{1,0:T(8,128)} async-done(((f32[256,256]{1,0:T(8,128)}), f32[32,256]{1,0:T(8,128)}) %reduce-scatter.3.cloned.1.call-update) | async-done | bytes 32784 | tf_op jit(solution)/shard_map/reduce_scatter | solution.py:68
  223.6 0.0 copy-done.6
  223.6 2.0 multiply_reduce_fusion
  226.9 0.1 copy.21
  227.1 40.1 %psum.7 = f32[]{:T(128)} all-reduce(f32[]{:T(128)S(6)} %add.44), channel_id=1, replica_groups=mesh['fs'=8,'tp'=4] {'fs','tp'}, use_global_device_ids=true, to_apply=%region_4.0 | all-reduce | flops 1 | bytes 8 | tf_op jit(solution)/shard_map/psum | solution.py:81
  267.9 30.8 %all_gather.19 = f32[256,256]{1,0:T(8,128)S(1)} all-gather(f32[32,256]{1,0:T(8,128)S(1)} %get-tuple-element.29), channel_id=1, replica_groups=mesh['fs'=8,'tp'=4] {'fs'}, dimensions={0}, use_global_device_ids=true | all-gather | bytes 294912 | tf_op jit(solution)/shard_map/all_gather | solution.py:78
  298.7 1.1 fusion.5
  299.7 0.0 all-gather.8.cloned.1.call-update
  299.7 0.1 copy.22
  299.8 30.9 %all_gather.21 = f32[256,128]{1,0:T(8,128)S(1)} all-gather(f32[32,128]{1,0:T(8,128)S(1)} %get-tuple-element.25), channel_id=1, replica_groups=mesh['fs'=8,'tp'=4] {'fs'}, dimensions={0}, use_global_device_ids=true | all-gather | bytes 147456 | tf_op jit(solution)/shard_map/all_gather | solution.py:79
  330.8 0.3 fusion.4
  331.1 31.5 %all_gather.23 = bf16[2048,128]{0,1:T(8,128)(2,1)S(1)} all-gather(bf16[256,128]{0,1:T(8,128)(2,1)S(1)} %get-tuple-element.20), channel_id=1, replica_groups=mesh['fs'=8,'tp'=4] {'fs'}, dimensions={0}, use_global_device_ids=true | all-gather | bytes 589824 | tf_op jit(solution)/shard_map/all_gather | solution.py:96
  362.6 1.0 copy.28
  363.6 0.8 copy.24
  364.4 0.8 copy.26
  365.1 0.8 copy.23
  366.0 0.8 copy.25
  366.8 2.3 copy.27
  (7 shorter events, 0.0 us)
Async XLA Ops:
  7.2 93.0 %copy-start = (bf16[2560,256]{1,0:T(8,128)(2,1)S(1)}, bf16[2560,256]{1,0:T(8,128)(2,1)}, u32[]{:S(2)}) copy-start(bf16[2560,256]{1,0:T(8,128)(2,1)} %param.12) | copy-start | bytes 3932164
  7.2 46.0 %all-gather.6.cloned.1.call-start = ((), (), s32[]{:S(2)}) async-start(), calls=%async_computation.4 | async-start | bytes 1179648 | tf_op jit(solution)/shard_map/all_gather | solution.py:46
  7.9 86.4 %all-gather.4.cloned.1.call-start = ((), (), s32[]{:S(2)}) async-start(), calls=%async_computation.2 | async-start | bytes 1179648 | tf_op jit(solution)/shard_map/all_gather | solution.py:41
  8.7 50.4 %copy-start.1 = (bf16[2560,128]{1,0:T(8,128)(2,1)S(1)}, bf16[2560,128]{1,0:T(8,128)(2,1)}, u32[]{:S(2)}) copy-start(bf16[2560,128]{1,0:T(8,128)(2,1)} %param.13) | copy-start | bytes 1966084
  8.7 150.0 %reduce-scatter.5.cloned.1.call-start = ((), (), s32[]{:S(2)}) async-start(), calls=%async_computation.5 | async-start | bytes 147456 | tf_op jit(solution)/shard_map/reduce_scatter | solution.py:69
  62.0 161.7 %reduce-scatter.3.cloned.1.call-start = ((), (), s32[]{:S(2)}) async-start(), calls=%async_computation.3 | async-start | bytes 294912 | tf_op jit(solution)/shard_map/reduce_scatter | solution.py:68
  100.2 58.5 %copy-start.8 = (f32[32,128]{1,0:T(8,128)S(1)}, f32[32,128]{1,0:T(8,128)}, u32[]{:S(2)}) copy-start(f32[32,128]{1,0:T(8,128)} %param.21) | copy-start | bytes 49156
  100.2 58.5 %copy-start.9 = (f32[32,128]{1,0:T(8,128)S(1)}, f32[32,128]{1,0:T(8,128)}, u32[]{:S(2)}) copy-start(f32[32,128]{1,0:T(8,128)} %param.20) | copy-start | bytes 49156
  100.2 123.4 %copy-start.6 = (f32[32,256]{1,0:T(8,128)S(1)}, f32[32,256]{1,0:T(8,128)}, u32[]{:S(2)}) copy-start(f32[32,256]{1,0:T(8,128)} %param.19) | copy-start | bytes 98308
  100.3 123.4 %copy-start.7 = (f32[32,256]{1,0:T(8,128)S(1)}, f32[32,256]{1,0:T(8,128)}, u32[]{:S(2)}) copy-start(f32[32,256]{1,0:T(8,128)} %param.18) | copy-start | bytes 98308
  100.3 126.6 %copy-start.4 = (f32[256,256]{1,0:T(8,128)S(1)}, f32[256,256]{1,0:T(8,128)}, u32[]{:S(2)}) copy-start(f32[256,256]{1,0:T(8,128)} %param.14) | copy-start | bytes 786436
  100.3 198.4 %copy-start.2 = (bf16[256,256]{1,0:T(8,128)(2,1)S(1)}, bf16[256,256]{1,0:T(8,128)(2,1)}, u32[]{:S(2)}) copy-start(bf16[256,256]{1,0:T(8,128)(2,1)} %param.16) | copy-start | bytes 393220
  100.3 199.4 %copy-start.5 = (f32[256,128]{1,0:T(8,128)S(1)}, f32[256,128]{1,0:T(8,128)}, u32[]{:S(2)}) copy-start(f32[256,128]{1,0:T(8,128)} %param.15) | copy-start | bytes 393220
  103.2 227.6 %copy-start.3 = (bf16[256,256]{1,0:T(8,128)(2,1)S(1)}, bf16[256,256]{1,0:T(8,128)(2,1)}, u32[]{:S(2)}) copy-start(bf16[256,256]{1,0:T(8,128)(2,1)} %param.17) | copy-start | bytes 393220
  103.3 263.5 %all-gather.8.cloned.1.call-start = ((), (), s32[]{:S(2)}) async-start(), calls=%async_computation.6 | async-start | bytes 1179648 | tf_op jit(solution)/shard_map/all_gather | solution.py:95
Sparse Core Ops, SparseCore 0:
  10.1 42.9 all-gather.5
  55.3 38.9 all-gather.3
  98.2 60.4 reduce-scatter.4
  162.5 61.0 reduce-scatter.2
  299.9 40.3 all-gather.7
where the time goes:
time: 376 us
  waiting for transfers between devices  197 us (52%)
  blocking collectives  133 us (35%)
  matrix products  19 us (5%)
  between operations  15.9 us (4%)
  local copies, waits for them, and re-layouts  6.72 us (2%)
  other arithmetic  3.92 us (1%)
    reduce_scatter x1, waiting for transfers between devices, on_device(): lax.psum_scatter(value_part, 'fs', scatter_dimension=0, tiled=True)  63 us
    reduce_scatter x1, waiting for transfers between devices, on_device(): lax.psum_scatter(query_part, 'fs', scatter_dimension=0, tiled=True)  55.4 us
    all_gather x1, waiting for transfers between devices, on_device(): lax.all_gather(query_factor, 'fs', axis=0, tiled=True)  44.4 us
    psum x1, blocking collectives, on_device(): lax.psum(jnp.sum(value_dir_own * value_dir_own) + jnp.sum(query_dir_own *...  40.1 us
    all_gather x1, waiting for transfers between devices, on_device(): lax.all_gather(value_factor, 'fs', axis=0, tiled=True)  32.3 us
    all_gather x1, blocking collectives, on_device(): lax.all_gather(query_master_new.astype(jnp.bfloat16), 'fs', axis=0, tiled...  31.5 us
    all_gather x1, blocking collectives, on_device(): lax.all_gather(query_dir_own, 'fs', axis=0, tiled=True)  30.9 us
    all_gather x1, blocking collectives, on_device(): lax.all_gather(value_dir_own, 'fs', axis=0, tiled=True)  30.8 us
  transfers between devices with their start and end apart: 5, of which 4 were waited for; matrix products, arithmetic and copies ran while one was open for 6% of the time, Pallas kernels for 0%

commit v1 on v0

--- a/solution.py
+++ b/solution.py
@@ -43,7 +43,9 @@
     )
     query_reduced = jnp.dot(
         saved_input,
-        lax.all_gather(query_factor, "fs", axis=0, tiled=True),
+        jnp.concatenate(
+            lax.all_to_all(jnp.stack([query_factor] * lax.axis_size("fs")), "fs", 0, 0), axis=0
+        ),
         preferred_element_type=jnp.float32,
     )
     value_part = (

time: 376 us -> 348 us (0.926)
  waiting for transfers between devices: 197 us -> 160 us
  starting transfers between devices: 0.2 us -> 7.44 us
    all_gather x1 -> x0, waiting for transfers between devices: 44.4 us -> none  [on_device(): lax.all_gather(query_factor, 'fs', axis=0, tiled=True)]
    all_to_all x0 -> x1, waiting for transfers between devices: none -> 29.1 us  [on_device(): lax.all_to_all(jnp.stack([query_factor] * lax.axis_size('fs')), 'fs', 0, 0)]
    all_gather x1, waiting for transfers between devices: 32.3 us -> 11.2 us  [on_device(): lax.all_gather(value_factor, 'fs', axis=0, tiled=True)]
    all_to_all x0 -> x1, starting transfers between devices: none -> 7.28 us  [on_device(): lax.all_to_all(jnp.stack([query_factor] * lax.axis_size('fs')), 'fs', 0, 0)]
  transfers between devices with their start and end apart: 5 -> 5, of which waited for: 4 -> 4; matrix products, arithmetic and copies ran while one was open for 6% -> 7% of each run, Pallas kernels for 0% -> 0%
where the time goes in v1:
time: 348 us
  waiting for transfers between devices  160 us (46%)
  blocking collectives  133 us (38%)
  matrix products  18.7 us (5%)
  between operations  15.9 us (5%)
  local copies, waits for them, and re-layouts  8.77 us (3%)
  starting transfers between devices  7.44 us (2%)
  other arithmetic  3.92 us (1%)
    reduce_scatter x1, waiting for transfers between devices, on_device(): lax.psum_scatter(value_part, 'fs', scatter_dimension=0, tiled=True)  63.1 us
    reduce_scatter x1, waiting for transfers between devices, on_device(): lax.psum_scatter(query_part, 'fs', scatter_dimension=0, tiled=True)  55.4 us
    psum x1, blocking collectives, on_device(): lax.psum(jnp.sum(value_dir_own * value_dir_own) + jnp.sum(query_dir_own *...  40.1 us
    all_gather x1, blocking collectives, on_device(): lax.all_gather(query_master_new.astype(jnp.bfloat16), 'fs', axis=0, tiled...  31.4 us
    all_gather x1, blocking collectives, on_device(): lax.all_gather(query_dir_own, 'fs', axis=0, tiled=True)  30.9 us
    all_gather x1, blocking collectives, on_device(): lax.all_gather(value_dir_own, 'fs', axis=0, tiled=True)  30.8 us
    all_to_all x1, waiting for transfers between devices, on_device(): lax.all_to_all(jnp.stack([query_factor] * lax.axis_size('fs')), 'fs', 0, 0)  29.1 us
    all_gather x1, waiting for transfers between devices, on_device(): lax.all_gather(value_factor, 'fs', axis=0, tiled=True)  11.2 us
  transfers between devices with their start and end apart: 5, of which 4 were waited for; matrix products, arithmetic and copies ran while one was open for 7% of the time, Pallas kernels for 0%

profile of v1, /device:TPU:0, one launch (start us, length us, event | category | flops | bytes accessed | tf_op | source)
XLA Modules:
  0.0 347.5 jit_solution(15840966946476995835)
XLA Ops:
  7.2 0.0 copy-start
  7.2 2.0 stack.2
  9.2 7.3 %all-to-all-start = ((bf16[8,256,256]{2,1,0:T(8,128)(2,1)}), bf16[8,256,256]{2,1,0:T(8,128)(2,1)S(1)}, u32[]{:S(2)}, u32[]{:S(2)}) async-start(bf16[8,256,256]{2,1,0:T(8,128)(2,1)} %stack.2), calls=%async_computation.1 | async-start | bytes 2097152 | tf_op jit(solution)/shard_map/all_to_all | solution.py:47
  16.5 0.0 all-gather.3.cloned.1.call-start
  16.6 0.7 all-gather.3.cloned.1.call-update
  17.3 0.0 reduce-scatter.5.cloned.1.call-start
  17.3 29.1 %all-to-all-done = bf16[8,256,256]{2,1,0:T(8,128)(2,1)S(1)} async-done(((bf16[8,256,256]{2,1,0:T(8,128)(2,1)}), bf16[8,256,256]{2,1,0:T(8,128)(2,1)S(1)}, u32[]{:S(2)}, u32[]{:S(2)}) %all-to-all-start) | async-done | bytes 1048608 | tf_op jit(solution)/shard_map/all_to_all | solution.py:47
  46.4 5.7 %fusion.9 = f32[2560,256]{1,0:T(8,128)S(1)} fusion(bf16[2560,2048]{1,0:T(8,128)(2,1)} %param.11, bf16[2048,256]{1,0:T(8,128)(2,1)S(1)} %bitcast.17), kind=kOutput, calls=%fused_computation.21 | convolution fusion | flops 2684354560 | bytes 14155776 | tf_op jit(solution)/shard_map/dot_general | solution.py:44
  52.1 0.0 copy-done.1
  52.1 2.9 convolution_multiply_fusion.3
  54.9 0.0 reduce-scatter.5.cloned.1.call-update
  55.0 0.0 reduce-scatter.3.cloned.1.call-start
  55.0 11.2 %all-gather.3.cloned.1.call-done = bf16[2048,256]{1,0:T(8,128)(2,1)} async-done(((bf16[256,256]{1,0:T(8,128)(2,1)}), bf16[2048,256]{1,0:T(8,128)(2,1)}) %all-gather.3.cloned.1.call-update) | async-done | bytes 1048592 | tf_op jit(solution)/shard_map/all_gather | solution.py:41
  66.2 5.9 %fusion.8 = f32[2560,256]{1,0:T(8,128)S(1)} fusion(bf16[2560,2048]{1,0:T(8,128)(2,1)} %param.11, bf16[2048,256]{1,0:T(8,128)(2,1)} %all-gather.3.cloned.1.call-done), kind=kOutput, calls=%fused_computation.20 | convolution fusion | flops 2684354560 | bytes 14155776 | tf_op jit(solution)/shard_map/dot_general | solution.py:39
  72.1 0.0 copy-done
  72.1 0.0 copy-start.8
  72.1 0.0 copy-start.9
  72.1 0.0 copy-start.6
  72.1 0.0 copy-start.7
  72.2 0.0 copy-start.4
  72.2 0.0 copy-start.3
  72.2 0.0 copy-start.5
  72.2 2.9 convolution_multiply_fusion.1
  75.1 0.0 reduce-scatter.3.cloned.1.call-update
  75.1 0.0 all-gather.5.cloned.1.call-start
  75.2 55.4 %reduce-scatter.5.cloned.1.call-done = f32[32,128]{1,0:T(8,128)} async-done(((f32[256,128]{1,0:T(8,128)}), f32[32,128]{1,0:T(8,128)}) %reduce-scatter.5.cloned.1.call-update) | async-done | bytes 16400 | tf_op jit(solution)/shard_map/reduce_scatter | solution.py:71
  130.6 0.0 copy-done.8
  130.6 1.9 multiply_reduce_fusion.1
  132.5 63.1 %reduce-scatter.3.cloned.1.call-done = f32[32,256]{1,0:T(8,128)} async-done(((f32[256,256]{1,0:T(8,128)}), f32[32,256]{1,0:T(8,128)}) %reduce-scatter.3.cloned.1.call-update) | async-done | bytes 32784 | tf_op jit(solution)/shard_map/reduce_scatter | solution.py:70
  195.7 0.0 copy-done.7
  195.7 2.0 multiply_reduce_fusion
  199.0 0.0 copy-done.4
  199.0 0.1 copy.21
  199.1 40.1 %psum.7 = f32[]{:T(128)} all-reduce(f32[]{:T(128)S(6)} %add.44), channel_id=1, replica_groups=mesh['fs'=8,'tp'=4] {'fs','tp'}, use_global_device_ids=true, to_apply=%region_4.0 | all-reduce | flops 1 | bytes 8 | tf_op jit(solution)/shard_map/psum | solution.py:83
  239.9 30.8 %all_gather.16 = f32[256,256]{1,0:T(8,128)S(1)} all-gather(f32[32,256]{1,0:T(8,128)S(1)} %get-tuple-element.29), channel_id=1, replica_groups=mesh['fs'=8,'tp'=4] {'fs'}, dimensions={0}, use_global_device_ids=true | all-gather | bytes 294912 | tf_op jit(solution)/shard_map/all_gather | solution.py:80
  270.7 0.0 copy-done.3
  270.7 1.1 fusion.5
  271.7 0.0 all-gather.5.cloned.1.call-update
  271.8 0.1 copy.22
  271.9 30.9 %all_gather.17 = f32[256,128]{1,0:T(8,128)S(1)} all-gather(f32[32,128]{1,0:T(8,128)S(1)} %get-tuple-element.25), channel_id=1, replica_groups=mesh['fs'=8,'tp'=4] {'fs'}, dimensions={0}, use_global_device_ids=true | all-gather | bytes 147456 | tf_op jit(solution)/shard_map/all_gather | solution.py:81
  302.8 0.3 fusion.4
  303.1 31.4 %all_gather.19 = bf16[2048,128]{0,1:T(8,128)(2,1)S(1)} all-gather(bf16[256,128]{0,1:T(8,128)(2,1)S(1)} %get-tuple-element.20), channel_id=1, replica_groups=mesh['fs'=8,'tp'=4] {'fs'}, dimensions={0}, use_global_device_ids=true | all-gather | bytes 589824 | tf_op jit(solution)/shard_map/all_gather | solution.py:98
  334.6 1.0 copy.28
  335.6 0.8 copy.24
  336.3 0.8 copy.26
  337.1 0.8 copy.23
  337.9 0.8 copy.25
  338.8 2.3 copy.27
  (7 shorter events, 0.0 us)
Async XLA Ops:
  7.2 64.9 %copy-start = (bf16[2560,256]{1,0:T(8,128)(2,1)S(1)}, bf16[2560,256]{1,0:T(8,128)(2,1)}, u32[]{:S(2)}) copy-start(bf16[2560,256]{1,0:T(8,128)(2,1)} %param.12) | copy-start | bytes 3932164
  9.2 37.2 %all-to-all-start = ((bf16[8,256,256]{2,1,0:T(8,128)(2,1)}), bf16[8,256,256]{2,1,0:T(8,128)(2,1)S(1)}, u32[]{:S(2)}, u32[]{:S(2)}) async-start(bf16[8,256,256]{2,1,0:T(8,128)(2,1)} %stack.2), calls=%async_computation.1 | async-start | bytes 2097152 | tf_op jit(solution)/shard_map/all_to_all | solution.py:47
  16.5 49.7 %all-gather.3.cloned.1.call-start = ((), (), s32[]{:S(2)}) async-start(), calls=%async_computation.3 | async-start | bytes 1179648 | tf_op jit(solution)/shard_map/all_gather | solution.py:41
  17.3 113.4 %reduce-scatter.5.cloned.1.call-start = ((), (), s32[]{:S(2)}) async-start(), calls=%async_computation.5 | async-start | bytes 147456 | tf_op jit(solution)/shard_map/reduce_scatter | solution.py:71
  46.4 5.7 %copy-start.1 = (bf16[2560,128]{1,0:T(8,128)(2,1)S(1)}, bf16[2560,128]{1,0:T(8,128)(2,1)}, u32[]{:S(2)}) copy-start(bf16[2560,128]{1,0:T(8,128)(2,1)} %param.13) | copy-start | bytes 1966084
  55.0 140.7 %reduce-scatter.3.cloned.1.call-start = ((), (), s32[]{:S(2)}) async-start(), calls=%async_computation.4 | async-start | bytes 294912 | tf_op jit(solution)/shard_map/reduce_scatter | solution.py:70
  72.1 58.5 %copy-start.8 = (f32[32,128]{1,0:T(8,128)S(1)}, f32[32,128]{1,0:T(8,128)}, u32[]{:S(2)}) copy-start(f32[32,128]{1,0:T(8,128)} %param.21) | copy-start | bytes 49156
  72.1 58.5 %copy-start.9 = (f32[32,128]{1,0:T(8,128)S(1)}, f32[32,128]{1,0:T(8,128)}, u32[]{:S(2)}) copy-start(f32[32,128]{1,0:T(8,128)} %param.20) | copy-start | bytes 49156
  72.1 123.5 %copy-start.6 = (f32[32,256]{1,0:T(8,128)S(1)}, f32[32,256]{1,0:T(8,128)}, u32[]{:S(2)}) copy-start(f32[32,256]{1,0:T(8,128)} %param.19) | copy-start | bytes 98308
  72.1 123.5 %copy-start.7 = (f32[32,256]{1,0:T(8,128)S(1)}, f32[32,256]{1,0:T(8,128)}, u32[]{:S(2)}) copy-start(f32[32,256]{1,0:T(8,128)} %param.18) | copy-start | bytes 98308
  72.2 126.8 %copy-start.4 = (f32[256,256]{1,0:T(8,128)S(1)}, f32[256,256]{1,0:T(8,128)}, u32[]{:S(2)}) copy-start(f32[256,256]{1,0:T(8,128)} %param.14) | copy-start | bytes 786436
  72.2 198.5 %copy-start.3 = (bf16[256,256]{1,0:T(8,128)(2,1)S(1)}, bf16[256,256]{1,0:T(8,128)(2,1)}, u32[]{:S(2)}) copy-start(bf16[256,256]{1,0:T(8,128)(2,1)} %param.16) | copy-start | bytes 393220
  72.2 199.6 %copy-start.5 = (f32[256,128]{1,0:T(8,128)S(1)}, f32[256,128]{1,0:T(8,128)}, u32[]{:S(2)}) copy-start(f32[256,128]{1,0:T(8,128)} %param.15) | copy-start | bytes 393220
  75.1 227.7 %copy-start.2 = (bf16[256,256]{1,0:T(8,128)(2,1)S(1)}, bf16[256,256]{1,0:T(8,128)(2,1)}, u32[]{:S(2)}) copy-start(bf16[256,256]{1,0:T(8,128)(2,1)} %param.17) | copy-start | bytes 393220
  75.1 263.6 %all-gather.5.cloned.1.call-start = ((), (), s32[]{:S(2)}) async-start(), calls=%async_computation.6 | async-start | bytes 1179648 | tf_op jit(solution)/shard_map/all_gather | solution.py:97
Sparse Core Ops, SparseCore 0:
  19.4 46.6 all-gather.2
  70.1 60.4 reduce-scatter.4
  134.5 61.0 reduce-scatter.2
  271.9 41.3 all-gather.4
